TPU v7x, 256 devices: a 4x2x16 block of a 4x16x16 slice. The times are simulated.
256 devices in a mesh: grp: 2 (over y), fs: 16 (over z), tp: 8 (over x, core).
Axes of the slice: x: 4, y: 2, z: 16, core: 2. Of those that a mesh axis runs over, the one named last changes fastest.
The devices are a block of a 4x16x16 slice.
Arguments:
- tokens: bfloat16 [32768, 2048], P(('grp', 'fs', 'tp')), parts along dimension 0, may hold values from -6 to 6
- first_gain: float32 [2048], replicated, may hold values from 0.1 to 1.9
- mixer_gain: float32 [2048], replicated, may hold values from 0.1 to 1.9
- gate_weight: bfloat16 [2048, 4608], P('fs', 'tp'), may hold values from -0.125 to 0.125
- up_weight: bfloat16 [2048, 4608], P('fs', 'tp'), may hold values from -0.125 to 0.125
- down_weight: bfloat16 [4608, 2048], P('tp', 'fs'), may hold values from -0.09375 to 0.09375
- query_weight: bfloat16 [2048, 2048], P('fs', 'tp'), may hold values from -0.125 to 0.125
- key_weight: bfloat16 [2048, 2048], P('fs', 'tp'), may hold values from -0.125 to 0.125
- value_weight: bfloat16 [2048, 4096], P('fs', 'tp'), may hold values from -0.125 to 0.125
- head_gain: float32 [4096], P('tp'), may hold values from 0.1 to 1.9
- out_weight: bfloat16 [4096, 2048], P('tp', 'fs'), may hold values from -0.09375 to 0.09375
- log_decay: float32 [2, 8], P(None, 'tp'), may hold values from -0.03125 to 0, as said below
Outputs:
- updated: bfloat16 [32768, 2048], P(('grp', 'fs', 'tp')), parts along dimension 0
There are 2 independent parts, one for each index of `grp`. A program takes and returns all parts, laid end to end along the dimension named above; an argument that names none is the same for every part. Nothing has to cross between parts.
Inputs may be any that keep to these rules, and one draw needn't show every extreme that they name: `log_decay`: log decay per step of each direction (forward, then backward) and head.
All inputs are finite; a program needn't handle non-finite values.
Results may differ from a plain program's by a relative error of at most 0.02.
Values may be sent and summed in bfloat16 or wider, within the bound.
A program may use at most 64 MiB of HBM per device.

v0:
```python
import jax
import jax.numpy as jnp
from jax import lax
from jax.sharding import PartitionSpec as P

DK = 256
DV = 512
BLOCK = 128


EPS = 1e-06


def side_by_side(arrays, axis, dim, along):
    ends, at = ([], 0)
    for a in arrays[:-1]:
        at += a.shape[along]
        ends.append(at)
    both = jnp.concatenate(arrays, axis=along)
    return tuple(jnp.split(lax.all_gather(both, axis, axis=dim, tiled=True), ends, axis=along))


def from_everyone(shard, axis):
    copies = jnp.broadcast_to(shard, (lax.axis_size(axis), *shard.shape))
    return lax.all_to_all(copies, axis, split_axis=0, concat_axis=0, tiled=True)


def laid_out(pieces, dim):
    lengths = list(pieces.shape[1:])
    lengths[dim] *= pieces.shape[0]
    return jnp.moveaxis(pieces, 0, dim).reshape(lengths)


def gathered_copies(shard, axis, dim):
    pieces = from_everyone(shard, axis)
    return laid_out(pieces, dim)


def in_blocks(shard, dim, length):
    before, after = (shard.shape[:dim], shard.shape[dim + 1 :])
    return jnp.moveaxis(shard.reshape(*before, length, -1, *after), dim, 0)


def sum_at_owner(shard, axis, dim):
    pieces = in_blocks(shard, dim, lax.axis_size(axis))
    arrived = lax.all_to_all(pieces, axis, split_axis=0, concat_axis=0, tiled=True)
    return arrived.astype(jnp.float32).sum(axis=0)


def norm_rows(values, gain):
    widened = values.astype(jnp.float32)
    factor = lax.rsqrt(jnp.mean(widened * widened, axis=-1, keepdims=True) + EPS)
    return (widened * factor * gain).astype(jnp.bfloat16)


def sweep_one(queries, key_rows, value_rows, log_rate):
    length = queries.shape[0]
    block_count = length // BLOCK
    places = jnp.arange(BLOCK, dtype=jnp.float32)
    distance = places[:, None] - places[None, :]
    inner_decay = jnp.where(distance >= 0, jnp.exp(log_rate * jnp.maximum(distance, 0.0)), 0.0)
    enter_decay = jnp.exp(log_rate * (places + 1.0))
    leave_decay = jnp.exp(log_rate * (BLOCK - 1.0 - places))
    block_decay = jnp.exp(log_rate * BLOCK)

    def advance(memory, blocks):
        query_block, key_block, value_block = blocks
        scores = (
            jnp.dot(
                query_block.astype(jnp.bfloat16),
                key_block.astype(jnp.bfloat16).T,
                preferred_element_type=jnp.float32,
            )
            * inner_decay
        )
        result = jnp.dot(scores, value_block)
        result = result + jnp.dot(query_block, memory) * enter_decay[:, None]
        memory = memory * block_decay + jnp.dot((key_block * leave_decay[:, None]).T, value_block)
        return (memory, result)

    start_memory = jnp.zeros((queries.shape[1], value_rows.shape[1]), jnp.float32)
    _, results = lax.scan(
        advance,
        start_memory,
        (
            queries.reshape(block_count, BLOCK, -1),
            key_rows.reshape(block_count, BLOCK, -1),
            value_rows.reshape(block_count, BLOCK, -1),
        ),
    )
    return results.reshape(length, -1)


def retain_both(queries, key_rows, value_rows, forward_rate, backward_rate):
    forward_part = sweep_one(queries, key_rows, value_rows, forward_rate)
    backward_part = sweep_one(
        jnp.flip(queries, axis=0),
        jnp.flip(key_rows, axis=0),
        jnp.flip(value_rows, axis=0),
        backward_rate,
    )
    return forward_part + jnp.flip(backward_part, axis=0)


def head_norm(outputs, gain):
    heads_here = gain.shape[0] // DV
    centered = outputs - jnp.mean(outputs, axis=-1, keepdims=True)
    variance = jnp.mean(centered * centered, axis=-1, keepdims=True)
    return centered * lax.rsqrt(variance + EPS) * gain.reshape(heads_here, 1, DV)


def to_heads(values, width):
    widened = lax.optimization_barrier(values.astype(jnp.bfloat16)).astype(jnp.float32)
    return widened.reshape(values.shape[0], -1, width).transpose(1, 0, 2)


def feed_half(residual, gain, gate_weight, up_weight, down_weight):
    normed = norm_rows(residual, gain)
    gathered = lax.all_gather(normed, "tp", axis=0, tiled=True)
    segments = side_by_side((gate_weight, up_weight), "fs", 0, 1)
    gate_sum = jnp.dot(gathered, segments[0], preferred_element_type=jnp.float32)
    up_sum = jnp.dot(gathered, segments[1], preferred_element_type=jnp.float32)
    hidden = (jax.nn.silu(gate_sum) * up_sum).astype(jnp.bfloat16)
    partial_out = jnp.dot(
        hidden, gathered_copies(down_weight, "fs", 1), preferred_element_type=jnp.float32
    )
    summed = sum_at_owner(partial_out.astype(jnp.bfloat16), "tp", 0)
    return (residual.astype(jnp.float32) + 0.5 * summed).astype(jnp.bfloat16)


def mix_tokens(residual, gain, head_gain, out_weight, log_decay, held):
    normed = norm_rows(residual, gain)
    gathered = lax.all_gather(normed, "tp", axis=0, tiled=True)
    rows_here = gathered.shape[0]
    query_sum = jnp.dot(gathered, held[0], preferred_element_type=jnp.float32)
    key_sum = jnp.dot(gathered, held[1], preferred_element_type=jnp.float32)
    value_sum = jnp.dot(gathered, held[2], preferred_element_type=jnp.float32)
    queries = to_heads(query_sum, DK) * DK ** (-0.5)
    key_rows = to_heads(key_sum, DK)
    value_rows = to_heads(value_sum, DV)
    outputs = jax.vmap(retain_both)(queries, key_rows, value_rows, log_decay[0], log_decay[1])
    normed_heads = head_norm(outputs, head_gain).astype(jnp.bfloat16)
    flat = normed_heads.transpose(1, 0, 2).reshape(rows_here, -1)
    partial_out = jnp.dot(
        flat,
        lax.all_gather(out_weight, "fs", axis=1, tiled=True),
        preferred_element_type=jnp.float32,
    )
    summed = sum_at_owner(partial_out.astype(jnp.bfloat16), "tp", 0)
    return (residual.astype(jnp.float32) + summed).astype(jnp.bfloat16)


def shards(
    tokens,
    first_gain,
    mixer_gain,
    gate_weight,
    up_weight,
    down_weight,
    query_weight,
    key_weight,
    value_weight,
    head_gain,
    out_weight,
    log_decay,
):
    held = side_by_side((query_weight, key_weight, value_weight), "fs", 0, 1)
    after_first = feed_half(tokens, first_gain, gate_weight, up_weight, down_weight)
    return mix_tokens(after_first, mixer_gain, head_gain, out_weight, log_decay, held)


def solution(mesh):
    placed = (
        P(("grp", "fs", "tp"), None),
        P(),
        P(),
        P("fs", "tp"),
        P("fs", "tp"),
        P("tp", "fs"),
        P("fs", "tp"),
        P("fs", "tp"),
        P("fs", "tp"),
        P("tp"),
        P("tp", "fs"),
        P(None, "tp"),
    )
    return jax.shard_map(
        shards, mesh=mesh, in_specs=placed, out_specs=P(("grp", "fs", "tp"), None), check_vma=False
    )
```

profile of v0, /device:TPU:33, one launch (start us, length us, event | category | flops | bytes accessed | tf_op | source)
XLA Modules:
  0.0 523.5 jit_solution(15582555828451249463)
XLA Ops:
  7.8 2.0 fusion.103
  13.6 24.6 %all-to-all-start = ((bf16[16,576,128]{2,1,0:T(8,128)(2,1)}), bf16[16,576,128]{2,1,0:T(8,128)(2,1)S(1)}, u32[]{:S(2)}, u32[]{:S(2)}) async-start(bf16[16,576,128]{2,1,0:T(8,128)(2,1)} %broadcast_in_dim.14), calls=%async_computation | async-start | bytes 4718592 | tf_op jit(solution)/shard_map/all_to_all | solution.py:25
  39.2 23.9 %all-gather.6.cloned.1.call-done = bf16[1024,2048]{1,0:T(8,128)(2,1)} async-done(((bf16[128,2048]{1,0:T(8,128)(2,1)}), bf16[1024,2048]{1,0:T(8,128)(2,1)}) %all-gather.6.cloned.1.call-update) | async-done | bytes 4194320 | tf_op jit(solution)/shard_map/all_gather | solution.py:119
  63.2 143.1 %all-gather.8.cloned.1.call-done = bf16[2048,1152]{0,1:T(8,128)(2,1)} async-done(((bf16[128,1152]{0,1:T(8,128)(2,1)}), bf16[2048,1152]{0,1:T(8,128)(2,1)}) %all-gather.8.cloned.1.call-update) | async-done | bytes 4718608 | tf_op jit(solution)/shard_map/all_gather | solution.py:20
  206.3 7.0 %fusion.92 = f32[1024,576]{0,1:T(8,128)} fusion(bf16[1024,2048]{1,0:T(8,128)(2,1)} %all-gather.6.cloned.1.call-done, bf16[2048,1152]{0,1:T(8,128)(2,1)} %all-gather.8.cloned.1.call-done), kind=kOutput, calls=%fused_computation.96 | convolution fusion | flops 2415919104 | bytes 8912896 | tf_op jit(solution)/shard_map/dot_general | solution.py:121
  213.3 10.3 %convolution_convert_fusion.1 = bf16[1024,2048]{1,0:T(8,128)(2,1)} fusion(f32[1024,576]{0,1:T(8,128)} %fusion.92, bf16[1024,2048]{1,0:T(8,128)(2,1)} %all-gather.6.cloned.1.call-done, bf16[2048,1152]{0,1:T(8,128)(2,1)} %all-gather.8.cloned.1.call-done, bf16[16,576,128]{2,1,0:T(8,128)(2,1)S(1)} %all-to-all-done), kind=kOutput, calls=%fused_computation.91 | convolution fusion | flops 4837474304 | bytes 15466496 | tf_op jit(solution)/shard_map/dot_general | solution.py:124
  223.7 63.9 %all_to_all.15 = bf16[8,128,2048]{2,1,0:T(8,128)(2,1)S(1)} all-to-all(bf16[8,128,2048]{2,1,0:T(8,128)(2,1)} %bitcast.175), channel_id=1, replica_groups=mesh['grp'=2,'fs'=16,'tp'=8] {'tp'}, dimensions={0} | all-to-all | bytes 8388608 | tf_op jit(solution)/shard_map/all_to_all | solution.py:46
  293.5 33.1 %all-gather.10.cloned.1.call-done = bf16[1024,2048]{1,0:T(8,128)(2,1)} async-done(((bf16[128,2048]{1,0:T(8,128)(2,1)}), bf16[1024,2048]{1,0:T(8,128)(2,1)}) %all-gather.10.cloned.1.call-update) | async-done | bytes 4194320 | tf_op jit(solution)/shard_map/all_gather | solution.py:133
  326.5 3.7 convolution_convert_fusion.3
  330.3 5.3 %reverse.10 = f32[1024,256]{1,0:T(8,128)} reverse(bf16[1024,256]{1,0:T(8,128)(2,1)S(1)} %convolution_convert_fusion.3), dimensions={0} | reverse | bytes 1572864 | tf_op jit(solution)/shard_map/reverse.1
  336.6 3.7 convolution_convert_fusion.2
  341.7 5.2 fusion.98
  347.0 10.3 %reverse.11 = bf16[1024,512]{1,0:T(8,128)(2,1)} reverse(bf16[1024,512]{1,0:T(8,128)(2,1)S(1)} %fusion.98), dimensions={0} | reverse | bytes 2097152 | tf_op jit(solution)/shard_map/reverse.2
  358.5 40.6 %while.31 = (s32[]{:T(128)}, f32[1,256,512]{2,1,0:T(8,128)S(1)}, f32[8,1,128,512]{3,2,1,0:T(8,128)S(1)}, f32[1]{0:T(128)}, f32[8,1,128,256]{3,2,1,0:T(8,128)}, /...) while((s32[]{:T(128)}, f32[1,256,512]{2,1,0:T(8,128)S(1)}, ...), condition=%wide.region_6.7_spmd.clone.clone.clone, body=%wide.region_5.6_spmd.clone.clone.clone.sunk | while | flops 93078016 | bytes 2955892 | solution.py:82
  360.2 2.0 fusion.164
  365.3 2.0 fusion.164
  370.4 2.0 fusion.164
  380.5 2.0 fusion.164
  385.6 2.0 fusion.164
  400.7 45.2 %while.30 = (s32[]{:T(128)}, f32[1,256,512]{2,1,0:T(8,128)S(1)}, f32[8,1,128,512]{3,2,1,0:T(8,128)}, f32[1]{0:T(128)}, f32[8,1,128,256]{3,2,1,0:T(8,128)}, /*ind...) while((s32[]{:T(128)}, f32[1,256,512]{2,1,0:T(8,128)S(1)}, ...), condition=%wide.region_4.5_spmd.clone.clone.clone, body=%wide.region_3.4_spmd.clone.clone.clone.sunk | while | flops 93078016 | bytes 2955892 | solution.py:82
  402.3 2.6 fusion.155
  408.0 2.6 fusion.155
  413.6 2.7 fusion.155
  419.3 2.7 fusion.155
  424.9 2.7 fusion.155
  430.6 2.7 fusion.155
  436.2 2.7 fusion.155
  441.9 2.7 fusion.155
  445.9 10.5 %rev.11 = f32[1,1024,512]{2,1,0:T(8,128)} reverse(f32[1,1024,512]{2,1,0:T(8,128)S(1)} %bitcast.171), dimensions={1} | reverse | bytes 4194304 | tf_op jit(solution)/shard_map/vmap(jit(_flip))/rev | solution.py:102
  456.4 2.5 fusion.119
  459.4 4.0 convolution_convert_fusion
  463.4 51.7 %all_to_all.16 = bf16[8,128,2048]{2,1,0:T(8,128)(2,1)S(1)} all-to-all(bf16[8,128,2048]{2,1,0:T(8,128)(2,1)S(1)} %bitcast.176), channel_id=1, replica_groups=mesh['grp'=2,'fs'=16,'tp'=8] {'tp'}, dimensions={0} | all-to-all | bytes 8388608 | tf_op jit(solution)/shard_map/all_to_all | solution.py:46
  (109 shorter events, 71.8 us)
Async XLA Ops:
  6.5 5.2 copy-start.4
  6.5 56.6 %all-gather.6.cloned.1.call-start = ((), (), s32[]{:S(2)}) async-start(), calls=%async_computation.3 | async-start | bytes 4718592 | tf_op jit(solution)/shard_map/all_gather | solution.py:119
  9.9 196.4 %all-gather.8.cloned.1.call-start = ((), (), s32[]{:S(2)}) async-start(), calls=%async_computation.4 | async-start | bytes 5013504 | tf_op jit(solution)/shard_map/all_gather | solution.py:20
  13.6 24.7 %copy-start.5 = (bf16[128,512]{1,0:T(8,128)(2,1)S(1)}, bf16[128,512]{1,0:T(8,128)(2,1)}, u32[]{:S(2)}) copy-start(bf16[128,512]{1,0:T(8,128)(2,1)} %param.24) | copy-start | bytes 393220
  13.6 24.7 %copy-start.6 = (bf16[128,256]{1,0:T(8,128)(2,1)S(1)}, bf16[128,256]{1,0:T(8,128)(2,1)}, u32[]{:S(2)}) copy-start(bf16[128,256]{1,0:T(8,128)(2,1)} %param.23) | copy-start | bytes 196612
  13.6 24.8 %copy-start.7 = (bf16[128,256]{1,0:T(8,128)(2,1)S(1)}, bf16[128,256]{1,0:T(8,128)(2,1)}, u32[]{:S(2)}) copy-start(bf16[128,256]{1,0:T(8,128)(2,1)} %param.22) | copy-start | bytes 196612
  13.6 199.7 %all-to-all-start = ((bf16[16,576,128]{2,1,0:T(8,128)(2,1)}), bf16[16,576,128]{2,1,0:T(8,128)(2,1)S(1)}, u32[]{:S(2)}, u32[]{:S(2)}) async-start(bf16[16,576,128]{2,1,0:T(8,128)(2,1)} %broadcast_in_dim.14), calls=%async_computation | async-start | bytes 4718592 | tf_op jit(solution)/shard_map/all_to_all | solution.py:25
  38.3 255.2 %all-gather.12.cloned.1.call-start = ((), (), s32[]{:S(2)}) async-start(), calls=%async_computation.6 | async-start | bytes 4456448 | tf_op jit(solution)/shard_map/all_gather | solution.py:20
  39.2 287.4 %all-gather.10.cloned.1.call-start = ((), (), s32[]{:S(2)}) async-start(), calls=%async_computation.5 | async-start | bytes 4718592 | tf_op jit(solution)/shard_map/all_gather | solution.py:133
  287.5 1.0 copy-start.1
  287.5 2.1 copy-start.8
  288.6 2.8 copy-start.9
  288.9 0.8 copy-start.2
  290.7 168.6 %all-gather.14.cloned.1.call-start = ((), (), s32[]{:S(2)}) async-start(), calls=%async_computation.7 | async-start | bytes 2228224 | tf_op jit(solution)/shard_map/all_gather | solution.py:146
  346.9 11.3 %copy-start = (bf16[1024,512]{1,0:T(8,128)(2,1)}, bf16[1024,512]{1,0:T(8,128)(2,1)S(1)}, u32[]{:S(2)}) copy-start(bf16[1024,512]{1,0:T(8,128)(2,1)S(1)} %fusion.98) | copy-start | bytes 3145732
  456.4 3.0 copy-start.10
  515.0 1.0 copy-start.3
Sparse Core Ops, SparseCore 0:
  10.0 53.0 all-gather.5
  64.9 141.3 all-gather.7
  208.1 72.4 all-gather.11
  290.8 35.6 all-gather.9
  328.1 65.7 all-gather.13
where the time goes:
time: 526 us; the launch traced here: 524 us
  waiting for transfers between devices  201 us (38%)
  blocking collectives  116 us (22%)
  matrix products  109 us (21%)
  local copies, waits for them, and re-layouts  32.4 us (6%)
  other arithmetic  25.6 us (5%)
  starting transfers between devices  25.1 us (5%)
  between operations  14.8 us (3%)
    all_gather x2, waiting for transfers between devices, side_by_side(): lax.all_gather(both, axis, axis=dim, tiled=True)  143 us
    all_to_all x2, blocking collectives, sum_at_owner(): lax.all_to_all(pieces, axis, split_axis=0, concat_axis=0, tiled=True)  116 us
    dot_general x16, matrix products, advance(): result = jnp.dot(scores, value_block)  37.4 us
    all_gather x1, waiting for transfers between devices, mix_tokens(): gathered = lax.all_gather(normed, 'tp', axis=0, tiled=True)  33.1 us
    all_to_all x1, starting transfers between devices, from_everyone(): return lax.all_to_all(copies, axis, split_axis=0, concat_axis=0, tiled=True)  24.6 us
    all_gather x1, waiting for transfers between devices, feed_half(): gathered = lax.all_gather(normed, 'tp', axis=0, tiled=True)  23.9 us
    dot_general x16, matrix products, advance(): jnp.dot((key_block * leave_decay[:, None]).T, value_block)  20.7 us
    another operation x5, local copies, waits for them, and re-layouts  18 us
  transfers between devices with their start and end apart: 6, of which 3 were waited for; matrix products, arithmetic and copies ran while one was open for 30% of the time, Pallas kernels for 0%

commit v1 on v0

v1 whole, which is shorter than its diff:
```python
import functools

import jax
import jax.numpy as jnp
from jax import lax
from jax.experimental import pallas as pl
from jax.experimental.pallas import tpu as pltpu
from jax.sharding import PartitionSpec as P

EPS = 1e-06
MESH = pl.DeviceIdType.MESH
F32, BF16 = jnp.float32, jnp.bfloat16
LANES = 128
ROW_TILE = 16
STEP_TILE = 512
PAIR_SHARE = (0.25, 0.34, 0.375, 0.3125)


def split_rows(rows, share):
    pair = int(rows * share) // ROW_TILE * ROW_TILE
    first = -(-(rows - pair) // (2 * ROW_TILE)) * ROW_TILE
    return first, rows - pair - first, pair


def half_mask(tile):
    return lax.broadcasted_iota(jnp.int32, tile.shape, 1) < LANES // 2


def kernel(
    sizes,
    tok_in,
    gain1,
    gain2,
    gate_in,
    up_in,
    down_in,
    q_in,
    k_in,
    v_in,
    hgain,
    out_in,
    rates,
    o_ref,
    gu,
    dn,
    qkv,
    wo,
    x1,
    x1n,
    acc,
    hid,
    p1,
    r1,
    s1,
    h1,
    f1,
    x2,
    p2,
    r2,
    s2,
    h2,
    f2,
    qs,
    ks,
    vs,
    decay,
    hn,
    ss,
    z_send,
    z_recv,
    y_send,
    y_recv,
    x_send,
    x_recv,
    a_send,
    a_recv,
    local_sem,
):
    n, groups = sizes
    half = n // 2
    d = n * LANES
    me = lax.axis_index("fs")
    r = lax.axis_index("tp")
    g = lax.axis_index("grp")
    up_z, down_z = lax.rem(me + 1, n), lax.rem(me + n - 1, n)
    x, c = r // 2, lax.rem(r, 2)
    xr, xl, xo = lax.rem(x + 1, 4), lax.rem(x + 3, 4), lax.rem(x + 2, 4)
    r_right, r_left, r_far = xr * 2 + c, xl * 2 + c, xo * 2 + c
    r_mate = x * 2 + 1 - c
    odd = lax.rem(g, 2)
    g_mate = g + 1 - 2 * odd
    rows = x1.shape[1]
    ff = gate_in.shape[1]
    main = ff // LANES * LANES
    tail = ff - main
    started = []

    def remote(src, dst, ss_, rs_, **to):
        return pltpu.make_async_remote_copy(
            src_ref=src, dst_ref=dst, send_sem=ss_, recv_sem=rs_, device_id=to, device_id_type=MESH
        )

    def send(ref, dst, ss_, rs_, **to):
        copy = remote(ref, dst, ss_, rs_, **to)
        copy.start()
        started.append(copy)

    def arrived(ref, ss_, rs_, **to):
        remote(ref, ref, ss_, rs_, **to).wait_recv()

    local = []

    def fetch(src, dst):
        copy = pltpu.make_async_copy(src, dst, local_sem.at[len(local)])
        copy.start()
        local.append(copy)

    fetch(tok_in, x1.at[r])
    fetch(down_in, dn.at[me, pl.ds(0, ff)])
    dk, dv = q_in.shape[1], v_in.shape[1]
    fetch(q_in, qkv.at[me, :, pl.ds(0, dk)])
    fetch(k_in, qkv.at[me, :, pl.ds(dk, dk)])
    fetch(v_in, qkv.at[me, :, pl.ds(2 * dk, dv)])
    fetch(out_in, wo.at[me])

    gu[me, :, :main] = gate_in[:, :main]
    gu[me, :, main : 2 * main] = up_in[:, :main]
    gu[me, :, 2 * main :] = jnp.concatenate([gate_in[:, main:], up_in[:, main:]], axis=1)

    barrier = pltpu.get_barrier_semaphore()
    neighbours = [
        {"fs": up_z},
        {"fs": down_z},
        {"tp": r_right},
        {"tp": r_left},
        {"tp": r_mate},
        {"grp": g_mate},
    ]
    for to in neighbours:
        pl.semaphore_signal(barrier, inc=1, device_id=to, device_id_type=MESH)
    pl.semaphore_wait(barrier, len(neighbours))
    for copy in local:
        copy.wait()

    kinds = (gu, dn, qkv, wo)
    lengths = (gu.shape[1], ff, qkv.shape[1], wo.shape[1])
    parts = [split_rows(length, share) for length, share in zip(lengths, PAIR_SHARE)]

    def z_rows(kind, sub):
        first, second, pair = parts[kind]
        if sub == 0:
            return pl.ds(pl.multiple_of(odd * (lengths[kind] - first), ROW_TILE), first)
        return pl.ds(pl.multiple_of(first + odd * (pair - first), ROW_TILE), second)

    def y_rows(kind, sent):
        pair = parts[kind][2]
        at = odd if sent else 1 - odd
        return pl.ds(pl.multiple_of(at * (lengths[kind] - pair), ROW_TILE), pair)

    def before(s):
        return lax.rem(me + n - s, n)

    def after(s):
        return lax.rem(me + s, n)

    def hops(sub, way):
        return half if sub == way else half - 1

    def z_start(kind, sub, way, s):
        block = before(s) if way == 0 else after(s)
        ref = kinds[kind].at[block, z_rows(kind, sub)]
        slot = (2 * kind + sub, way, s)
        send(ref, ref, z_send.at[slot], z_recv.at[slot], fs=up_z if way == 0 else down_z)

    def z_event(kind, sub, s):
        for way in range(2):
            if s > hops(sub, way):
                continue
            block = before(s) if way == 0 else after(s)
            ref = kinds[kind].at[block, z_rows(kind, sub)]
            slot = (2 * kind + sub, way, s - 1)
            arrived(ref, z_send.at[slot], z_recv.at[slot], fs=down_z if way == 0 else up_z)
            if s < hops(sub, way):
                z_start(kind, sub, way, s)
            if sub == 0:
                ref = kinds[kind].at[block, y_rows(kind, True)]
                slot = (kind, way, s - 1)
                send(ref, ref, y_send.at[slot], y_recv.at[slot], grp=g_mate)

    def y_wait(kind, s):
        for way in range(2):
            if s > hops(0, way):
                continue
            block = before(s) if way == 0 else after(s)
            ref = kinds[kind].at[block, y_rows(kind, False)]
            slot = (kind, way, s - 1)
            arrived(ref, y_send.at[slot], y_recv.at[slot], grp=g_mate)

    def pair_of(s):
        return (before(s), after(s)) if s < half else (me, after(half))

    def gather_start(buf, k):
        ref = buf(r)
        for i, to in enumerate((r_right, r_left, r_mate)):
            send(ref, ref, a_send.at[k, i], a_recv.at[k, i], tp=to)

    def gather_on(buf, k, count):
        for i, (src, onward) in enumerate(((r_left, r_right), (r_right, r_left))):
            ref = buf(src)
            arrived(ref, a_send.at[k, i], a_recv.at[k, i], tp=src)
            part = buf(src, pl.ds(i * (count // 2), count // 2))
            send(part, part, a_send.at[k, 3 + i], a_recv.at[k, 3 + i], tp=onward)
            send(ref, ref, a_send.at[k, 5 + i], a_recv.at[k, 5 + i], tp=r_mate)

    def gather_far(buf, k, count):
        for i, src in enumerate((r_left, r_right)):
            part = buf(r_far, pl.ds(i * (count // 2), count // 2))
            arrived(part, a_send.at[k, 3 + i], a_recv.at[k, 3 + i], tp=src)
        ref = buf(r_far)
        send(ref, ref, a_send.at[k, 7], a_recv.at[k, 7], tp=r_mate)

    def gather_mate(buf, k):
        for i, src in ((2, x), (5, xl), (6, xr), (7, xo)):
            ref = buf(src * 2 + 1 - c)
            arrived(ref, a_send.at[k, i], a_recv.at[k, i], tp=r_mate)

    def x1_buf(block, part=None):
        return x1.at[block] if part is None else x1.at[block, part]

    def x2_buf(q):
        def buf(block, part=None):
            return x2.at[q, block] if part is None else x2.at[q, block, part]

        return buf

    def sum_start(phase, q):
        p_, r_ = (p1, r1) if phase == 0 else (p2, r2)
        send(p_.at[q, 1 - c], r_.at[q], x_send.at[phase, q, 0], x_recv.at[phase, q, 0], tp=r_mate)

    def sum_chip(phase, q):
        p_, r_, s_, h_ = (p1, r1, s1, h1) if phase == 0 else (p2, r2, s2, h2)
        arrived(r_.at[q], x_send.at[phase, q, 0], x_recv.at[phase, q, 0], tp=r_mate)

        def add(to):
            s_[q, to] = (p_[q, c, to].astype(F32) + r_[q, to].astype(F32)).astype(BF16)

        add(xo)
        for i, to in enumerate((r_right, r_left)):
            part = pl.ds(i * (rows // 2), rows // 2)
            send(s_.at[q, xo, part], h_.at[q, i], x_send.at[phase, q, 1 + i], x_recv.at[phase, q, 1 + i], tp=to)
        add(xr)
        add(xl)
        add(x)

    def sum_on(phase, q):
        s_, h_, f_ = (s1, h1, f1) if phase == 0 else (s2, h2, f2)
        for i, (src, to, x_to) in enumerate(((r_left, r_right, xr), (r_right, r_left, xl))):
            arrived(h_.at[q, i], x_send.at[phase, q, 1 + i], x_recv.at[phase, q, 1 + i], tp=src)
            part = pl.ds(i * (rows // 2), rows // 2)
            s_[q, x_to, part] = (s_[q, x_to, part].astype(F32) + h_[q, i].astype(F32)).astype(BF16)
            send(s_.at[q, x_to], f_.at[q, i], x_send.at[phase, q, 3 + i], x_recv.at[phase, q, 3 + i], tp=to)

    def sum_end(phase, q):
        s_, f_ = (s1, f1) if phase == 0 else (s2, f2)
        for i, src in enumerate((r_left, r_right)):
            arrived(f_.at[q, i], x_send.at[phase, q, 3 + i], x_recv.at[phase, q, 3 + i], tp=src)
        return s_[q, x].astype(F32) + f_[q, 0].astype(F32) + f_[q, 1].astype(F32)

    def block_lanes(block):
        return pl.ds(pl.multiple_of(block * LANES, LANES), LANES)

    def blocks_of(q):
        per = STEP_TILE // LANES // 2
        return [b for s in range(q * per + 1, (q + 1) * per + 1) for b in pair_of(s)]

    def after_first(q):
        total = sum_end(0, q)
        for i, block in enumerate(blocks_of(q)):
            cols = slice(i * LANES, (i + 1) * LANES)
            base = x1[r, :, block_lanes(block)].astype(F32)
            x2[q, r, :, cols] = (base + 0.5 * total[:, cols]).astype(BF16)
        gather_start(x2_buf(q), 1 + q)

    def updated(q):
        total = sum_end(1, q) + x2[q, r].astype(F32)
        for i, block in enumerate(blocks_of(q)):
            o_ref[:, block_lanes(block)] = total[:, i * LANES : (i + 1) * LANES].astype(BF16)

    seq = x1n.shape[1]
    tile = seq // 2

    def norm_tokens(first, last):
        def body(i, carry):
            value = x1[i].astype(F32)
            factor = lax.rsqrt(jnp.mean(value * value, axis=1, keepdims=True) + EPS)
            value = (value * factor * gain1[...]).astype(BF16)
            to = pl.ds(pl.multiple_of(i * rows, rows), rows)
            for b in range(n):
                x1n[b, to] = value[:, b * LANES : (b + 1) * LANES]
            return carry

        lax.fori_loop(first, last, body, 0)

    def tiles(step, count=2):
        def body(m, carry):
            step(m)
            return carry

        lax.fori_loop(0, count, body, 0)

    def gu_compute(s):
        y_wait(0, s)
        a, b = pair_of(s)

        def step(m):
            part = pl.ds(pl.multiple_of(m * tile, tile), tile)
            left = jnp.concatenate([x1n[a, part], x1n[b, part]], axis=1)
            right = jnp.concatenate([gu[a], gu[b]], axis=0)
            product = jnp.dot(left, right, preferred_element_type=F32)
            acc[part] = product if s == 1 else acc[part] + product

        tiles(step)

    def silu_times(gate, up_value):
        return gate / (1.0 + jnp.exp(-gate)) * up_value

    def hidden():
        size = seq // 8

        def step(m):
            part = pl.ds(pl.multiple_of(m * size, size), size)
            hid[part, :main] = silu_times(acc[part, :main], acc[part, main : 2 * main]).astype(BF16)
            last = acc[part, 2 * main :]
            value = silu_times(last, pltpu.roll(last, LANES // 2, 1))
            hid[part, main:] = jnp.where(half_mask(value), value, 0.0).astype(BF16)

        tiles(step, 8)

    def project(kind, s, left, p_):
        y_wait(kind, s)
        a, b = pair_of(s)
        w = kinds[kind]
        q, at = (s - 1) // 2, (s - 1) % 2 * 2 * LANES

        def step(m):
            part = pl.ds(pl.multiple_of(m * tile, tile), tile)
            right = jnp.concatenate([w[a], w[b]], axis=1)
            product = jnp.dot(left[part], right, preferred_element_type=F32).astype(BF16)
            for i in range(tile // rows):
                to = m * (tile // rows // 2) + i // 2
                p_[q, i % 2, to, :, at : at + 2 * LANES] = product[i * rows : (i + 1) * rows]

        tiles(step)

    def qkv_compute(s):
        y_wait(2, s)
        a, b = pair_of(s)
        q, at = (s - 1) // 2, (s - 1) % 2 * 2 * LANES
        gain = jnp.concatenate([gain2[:, block_lanes(a)], gain2[:, block_lanes(b)]], axis=1)
        per = tile // rows
        width = qkv.shape[2]

        def step(m):
            part = pl.ds(pl.multiple_of(m * tile, tile), tile)
            value = x2[q, pl.ds(m * per, per), :, at : at + 2 * LANES].reshape(tile, 2 * LANES).astype(F32)
            square = value * value
            square = square[:, :LANES] + square[:, LANES:]
            right = jnp.concatenate([qkv[a], qkv[b]], axis=0)
            product = jnp.dot((value * gain).astype(BF16), right, preferred_element_type=F32)
            acc[part, :width] = product if s == 1 else acc[part, :width] + product
            ss[part] = square if s == 1 else ss[part] + square

        tiles(step)

    def qkv_end():
        size = seq // 4
        scale = dk**-0.5

        def step(m):
            part = pl.ds(pl.multiple_of(m * size, size), size)
            factor = lax.rsqrt(jnp.sum(ss[part], axis=1, keepdims=True) / d + EPS)
            qs[part] = ((acc[part, :dk] * factor).astype(BF16).astype(F32) * scale).astype(BF16)
            ks[part] = (acc[part, dk : 2 * dk] * factor).astype(BF16)
            vs[part] = (acc[part, 2 * dk : 2 * dk + dv] * factor).astype(BF16)

        tiles(step, 4)

    def make_decay(first, last):
        size = seq // 8
        forward, backward = rates[0, 0], rates[1, 0]

        def body(m, carry):
            at = lax.broadcasted_iota(jnp.int32, (size, seq), 0) + m * size
            gap = at - lax.broadcasted_iota(jnp.int32, (size, seq), 1)
            far = gap.astype(F32)
            weight = jnp.exp(jnp.where(gap >= 0, forward * far, -backward * far))
            decay[pl.ds(pl.multiple_of(m * size, size), size)] = jnp.where(gap == 0, 2.0, weight)
            return carry

        lax.fori_loop(first, last, body, 0)

    def retention():
        size = seq // 4

        def step(m):
            part = pl.ds(pl.multiple_of(m * size, size), size)
            score = lax.dot_general(qs[part], ks[...], (((1,), (1,)), ((), ())), preferred_element_type=F32)
            kept = jnp.dot((score * decay[part]).astype(BF16), vs[...], preferred_element_type=F32)
            kept = kept - jnp.mean(kept, axis=1, keepdims=True)
            variance = jnp.mean(kept * kept, axis=1, keepdims=True)
            hn[part] = (kept * lax.rsqrt(variance + EPS) * hgain[...]).astype(BF16)

        tiles(step, 4)

    def clear_padding():
        pad = dn.shape[1] - ff

        def body(i, carry):
            dn[i, ff:] = jnp.zeros((pad, LANES), BF16)
            return carry

        if pad:
            lax.fori_loop(0, n, body, 0)

    plan = []

    def at(place, what, *args):
        plan.append((place, len(plan), functools.partial(what, *args)))

    def ring_starts(place, kind, sub):
        for way in range(2):
            at(place, z_start, kind, sub, way, 0)

    place = {}
    order = [(0, sub, s) for s in range(1, half + 1) for sub in range(2)]
    for s in range(1, half + 1):
        order += [(1, 0, s), (2, 0, s), (1, 1, s)]
    lag = 3
    for slot in range(1, half + 1 + lag):
        if slot <= half:
            order.append((2, 1, slot))
        if slot > lag:
            order += [(3, 0, slot - lag), (3, 1, slot - lag)]
    for i, event in enumerate(order):
        place[event] = i
        at(i, z_event, *event)
    for kind in range(4):
        for sub in range(2):
            ring_starts(-1 if kind == 0 else place[kind, sub, 1] - 2.5, kind, sub)

    at(-0.9, gather_start, x1_buf, 0)
    at(-0.5, clear_padding)
    for i in range(4):
        at(0.5 + i, make_decay, 2 * i, 2 * i + 2)
    at(4.5, gather_on, x1_buf, 0, rows)
    at(6.5, gather_far, x1_buf, 0, rows)
    at(7.5, gather_mate, x1_buf, 0)
    at(7.6, norm_tokens, 0, 4)
    at(8.6, norm_tokens, 4, 8)
    when = 9.5
    for s in range(1, half + 1):
        when = max(when + 0.5, place[0, 1, s] + 1.5)
        at(when, gu_compute, s)
    at(when + 0.1, hidden)
    when += 0.2
    chunks = d // STEP_TILE
    per = half // chunks
    gathered = []
    for q in range(chunks):
        for s in range(q * per + 1, (q + 1) * per + 1):
            when = max(when + 0.5, place[1, 1, s] + 1.5)
            at(when, project, 1, s, hid, p1)
        at(when + 0.1, sum_start, 0, q)
        at(when + 2.2, sum_chip, 0, q)
        at(when + 5.2, sum_on, 0, q)
        at(when + 8.2, after_first, q)
        at(when + 11.2, gather_on, x2_buf(q), 1 + q, rows)
        at(when + 13.2, gather_far, x2_buf(q), 1 + q, rows)
        at(when + 14.2, gather_mate, x2_buf(q), 1 + q)
        gathered.append(when + 14.2)
    when = 0
    for s in range(1, half + 1):
        when = max(when + 0.5, place[2, 1, s] + 1.5, gathered[(s - 1) // per] + 0.1)
        at(when, qkv_compute, s)
    at(when + 0.1, qkv_end)
    at(when + 0.2, retention)
    when += 0.3
    for q in range(chunks):
        for s in range(q * per + 1, (q + 1) * per + 1):
            when = max(when + 0.5, place[3, 1, s] + 1.5)
            at(when, project, 3, s, hn, p2)
        at(when + 0.1, sum_start, 1, q)
        at(when + 1.2, sum_chip, 1, q)
        at(when + 2.2, sum_on, 1, q)
        at(when + 3.2, updated, q)

    for _, _, what in sorted(plan, key=lambda entry: entry[:2]):
        what()
    for copy in started:
        copy.wait_send()


def solution(mesh):
    n, n_tp, groups = mesh.shape["fs"], mesh.shape["tp"], mesh.shape["grp"]

    def shards(tokens, g1, g2, gate, up, down, query, key, value, head_gain, out, log_decay):
        rows, d = tokens.shape
        ff = gate.shape[1]
        dk, dv = query.shape[1], value.shape[1]
        seq = rows * n_tp
        chunks = d // STEP_TILE
        ff_pad = -(-ff // LANES) * LANES
        vmem = pl.BlockSpec(memory_space=pltpu.VMEM)
        hbm = pl.BlockSpec(memory_space=pl.ANY)
        sums = [
            pltpu.VMEM((chunks, 2, n_tp // 2, rows, STEP_TILE), BF16),
            pltpu.VMEM((chunks, n_tp // 2, rows, STEP_TILE), BF16),
            pltpu.VMEM((chunks, n_tp // 2, rows, STEP_TILE), BF16),
            pltpu.VMEM((chunks, 2, rows // 2, STEP_TILE), BF16),
            pltpu.VMEM((chunks, 2, rows, STEP_TILE), BF16),
        ]
        dma = pltpu.SemaphoreType.DMA
        return pl.pallas_call(
            functools.partial(kernel, (n, groups)),
            out_shape=jax.ShapeDtypeStruct((rows, d), BF16),
            in_specs=[hbm, vmem, vmem, vmem, vmem, hbm, hbm, hbm, hbm, vmem, hbm, pl.BlockSpec(memory_space=pltpu.SMEM)],
            out_specs=vmem,
            scratch_shapes=[
                pltpu.VMEM((n, LANES, 2 * ff), BF16),
                pltpu.VMEM((n, ff_pad, LANES), BF16),
                pltpu.VMEM((n, LANES, 2 * dk + dv), BF16),
                pltpu.VMEM((n, dv, LANES), BF16),
                pltpu.VMEM((n_tp, rows, d), BF16),
                pltpu.VMEM((n, seq, LANES), BF16),
                pltpu.VMEM((seq, 2 * ff), F32),
                pltpu.VMEM((seq, ff_pad), BF16),
                *sums,
                pltpu.VMEM((chunks, n_tp, rows, STEP_TILE), BF16),
                *sums,
                pltpu.VMEM((seq, dk), BF16),
                pltpu.VMEM((seq, dk), BF16),
                pltpu.VMEM((seq, dv), BF16),
                pltpu.VMEM((seq, seq), F32),
                pltpu.VMEM((seq, dv), BF16),
                pltpu.VMEM((seq, LANES), F32),
                dma((8, 2, n // 2)),
                dma((8, 2, n // 2)),
                dma((4, 2, n // 2)),
                dma((4, 2, n // 2)),
                dma((2, chunks, 5)),
                dma((2, chunks, 5)),
                dma((1 + chunks, 8)),
                dma((1 + chunks, 8)),
                dma((6,)),
            ],
            compiler_params=pltpu.CompilerParams(
                collective_id=0, has_side_effects=True, vmem_limit_bytes=67_000_000
            ),
        )(
            tokens,
            g1.reshape(1, -1),
            g2.reshape(1, -1),
            gate,
            up,
            down,
            query,
            key,
            value,
            head_gain.reshape(1, -1),
            out,
            log_decay,
        )

    placed = (
        P(("grp", "fs", "tp"), None),
        P(),
        P(),
        P("fs", "tp"),
        P("fs", "tp"),
        P("tp", "fs"),
        P("fs", "tp"),
        P("fs", "tp"),
        P("fs", "tp"),
        P("tp"),
        P("tp", "fs"),
        P(None, "tp"),
    )
    return jax.shard_map(
        shards, mesh=mesh, in_specs=placed, out_specs=P(("grp", "fs", "tp"), None), check_vma=False
    )
```

time: 526 us -> 195 us (0.37)
  waiting for transfers between devices: 201 us -> 0 us
  Pallas kernels: 0 us -> 189 us
  blocking collectives: 116 us -> 0 us
  matrix products: 109 us -> 0 us
  local copies, waits for them, and re-layouts: 32.4 us -> 5.72 us
  other arithmetic: 25.6 us -> 0 us
  starting transfers between devices: 25.1 us -> 0 us
  between operations: 14.8 us -> 0.01 us
    all_gather x5 -> x0, waiting for transfers between devices: 200 us -> none  [the longest x2 143 us: side_by_side(): lax.all_gather(both, axis, axis=dim, tiled=True)]
    pallas_call x0 -> x1, Pallas kernels: none -> 189 us  [shards(): pl.pallas_call(functools.partial(kernel, (n, groups)), out_shape=jax.Shap...]
    all_to_all x2 -> x0, blocking collectives: 116 us -> none  [sum_at_owner(): lax.all_to_all(pieces, axis, split_axis=0, concat_axis=0, tiled=True)]
    dot_general x54 -> x0, matrix products: 109 us -> none  [the longest x16 37.4 us: advance(): result = jnp.dot(scores, value_block)]
    all_to_all x1 -> x0, starting transfers between devices: 24.6 us -> none  [from_everyone(): return lax.all_to_all(copies, axis, split_axis=0, concat_axis=0, tiled=True)]
    another operation x5 -> x0, local copies, waits for them, and re-layouts: 18 us -> none
    mul x17 -> x0, other arithmetic: 11.4 us -> none  [the longest x16 10.5 us: advance(): result = result + jnp.dot(query_block, memory) * enter_decay[:, None]]
    rev x1 -> x0, local copies, waits for them, and re-layouts: 10.5 us -> none  [retain_both(): return forward_part + jnp.flip(backward_part, axis=0)]
  transfers between devices with their start and end apart: 6 -> 0, of which waited for: 3 -> 0; matrix products, arithmetic and copies ran while one was open for 30% -> 0% of each run, Pallas kernels for 0% -> 0%
where the time goes in v1:
time: 195 us; the launch traced here: 194 us
  Pallas kernels  189 us (97%)
  local copies, waits for them, and re-layouts  5.72 us (3%)
    pallas_call x1, Pallas kernels, shards(): pl.pallas_call(functools.partial(kernel, (n, groups)), out_shape=jax.Shap...  189 us
    unnamed x8, local copies, waits for them, and re-layouts  5.72 us

profile of v1, /device:TPU:33, one launch (start us, length us, event | category | flops | bytes accessed | tf_op | source)
XLA Modules:
  0.0 194.4 jit_solution(757908487496058434)
XLA Ops:
  0.0 0.0 copy-start.1
  0.0 0.7 copy-done.1
  0.7 0.6 copy.15.rates
  1.3 0.0 copy-start
  1.3 1.7 copy.13.gate_in
  3.0 0.0 copy-done
  3.0 0.8 copy.14.up_in
  3.8 188.7 %shard_map.118 = bf16[128,2048]{1,0:T(8,128)(2,1)} custom-call(bf16[128,2048]{1,0:T(8,128)(2,1)} %tok_in.1, f32[1,2048]{1,0:T(1,128)} %bitcast.3, f32[1,2048]{1,0:T(1,128)} %bitcast.4, bf16[128,576]{1,0:T(8,128)(2,1)} %copy.13.gate_in, bf16[128,576]{1,0:T(8,128)(2,1)} %copy.14.up_in, bf16[576,128]{1,0:T(8,128)(2,1)} %down_in.1, bf16[128,256]{1,0:T(8,128)(2,1)} %q_in.1, ...), custom_call_target="tpu_custom_call" | custom-call | tf_op jit(solution)/shard_map/pallas_call | solution.py:523
  192.5 1.9 copy.17
Async XLA Ops:
  0.0 0.7 copy-start.1
  1.3 1.8 copy-start

commit v2 on v1

--- a/solution.py
+++ b/solution.py
@@ -12,14 +12,123 @@
 F32, BF16 = jnp.float32, jnp.bfloat16
 LANES = 128
 ROW_TILE = 16
-STEP_TILE = 512
-PAIR_SHARE = (0.25, 0.34, 0.375, 0.3125)
+STEP_TILE = 256
+SHORTER = ((0, 1), (1, 0), (0, 1), (0, 1))
+PAIR_SHARE = (0.36, 0.43, 0.36, 0.36)
+RING_STARTS = ((((0, 0, 4),), ((0, 0, 6),)), (((1, 1, 2),), ((1, 1, 3),)), (((2, 0, 5),), ((1, 1, 8),)))
+RANKS = {}
+GU_TIME = 1.07
+LINK, MATE = 46650.0, 600000.0
+LATENCY = {"z0": 2.0, "z1": 2.0, "x0": 2.0, "x1": 2.0, "m": 1.1, "y": 2.0}
 
 
 def split_rows(rows, share):
     pair = int(rows * share) // ROW_TILE * ROW_TILE
-    first = -(-(rows - pair) // (2 * ROW_TILE)) * ROW_TILE
+    first = max(-(-(rows - pair) // (2 * ROW_TILE)) * ROW_TILE, pair)
     return first, rows - pair - first, pair
+
+
+def actions(sizes):
+    half, parts, row_bytes, hops = (sizes[k] for k in ("half", "parts", "row_bytes", "hops"))
+    per, chunk = sizes["per"], sizes["chunk_bytes"]
+    lasts = [per * (q + 1) for q in range(half // per)]
+    acts = {}
+
+    def act(name, rank, time, after=(), need=(), sends=()):
+        acts[name] = (RANKS.get(name[0], rank), time, list(after), list(need), list(sends))
+
+    def ways(kind, s):
+        return [w for w in range(2) if s <= hops[kind][w]]
+
+    def over_pair(kind, s):
+        return [("y", kind, w, s) for w in ways(kind, s)]
+
+    for kind in range(4):
+        nbytes = [rows * row_bytes[kind] for rows in parts[kind]]
+        for sub in range(2):
+            after = [("z_event", *v) for v in RING_STARTS[kind - 1][sub]] if kind else []
+            own = [(f"z{w}", nbytes[sub], ("z", kind, sub, w, 1)) for w in range(2)]
+            act(("z_own", kind, sub), -10 + 0.1 * kind, 0.03, after, (), own)
+            for s in range(1, half + 1):
+                need = [("z", kind, sub, w, s) for w in ways(kind, s)]
+                onward = [(f"z{w}", nbytes[sub], ("z", kind, sub, w, s + 1)) for w in ways(kind, s + 1)]
+                after = [("z_event", kind, sub, s - 1) if s > 1 else ("z_own", kind, sub)]
+                act(("z_event", kind, sub, s), -20 + kind, 0.05, after, need, onward)
+        for s in range(1, half + 1):
+            after = [("z_event", kind, 0, s)]
+            if s > 1 or kind:
+                after.append(("y_start", kind, s - 1) if s > 1 else ("y_start", kind - 1, half))
+            act(("y_start", kind, s), -15 + kind, 0.02, after, (), [("y", nbytes[2], v) for v in over_pair(kind, s)])
+
+    def gather(k, nbytes, first, rank):
+        on = [("x0", nbytes / 2, 3), ("m", nbytes, 5), ("x1", nbytes / 2, 4), ("m", nbytes, 6)]
+        for name, time, after, need, sends in (
+            ("gather_on", 0.05, first, (0, 1), on),
+            ("gather_far", 0.03, ("gather_on", k), (3, 4), [("m", nbytes, 7)]),
+            ("gather_mate", 0.01, ("gather_far", k), (2, 5, 6, 7), []),
+        ):
+            tags = [("g", k, i) for i in need]
+            act((name, k), rank, time, [after], tags, [(a, b, ("g", k, i)) for a, b, i in sends])
+        return [(to, nbytes, ("g", k, i)) for i, to in enumerate(("x0", "x1", "m"))]
+
+    sends = gather(0, sizes["tok_bytes"], ("gather_start", 0), -5)
+    act(("gather_start", 0), -30, 0.06, (), (), sends)
+    act(("clear_padding",), 50, 0.09)
+    decays = [("make_decay", 2 * i, 2 * i + 2) for i in range(4)]
+    for name in decays:
+        act(name, 60, 0.36)
+    norms = [("norm_tokens", 0, 4), ("norm_tokens", 4, 8)]
+    for name in norms:
+        act(name, -3, 0.92, [("gather_mate", 0)])
+    for s in range(1, half + 1):
+        after = [("z_event", 0, sub, s) for sub in range(2)] + (norms if s == 1 else [("gu_compute", s - 1)])
+        act(("gu_compute", s), 0, GU_TIME, after, over_pair(0, s))
+    act(("hidden",), 0, 0.85, [("gu_compute", half)])
+    for phase in range(2):
+        kind = 3 if phase else 1
+        first = ("retention",) if phase else ("hidden",)
+        for s in range(1, half + 1):
+            after = [("z_event", kind, sub, s) for sub in range(2)] + [("project", phase, s - 1) if s > 1 else first]
+            act(("project", phase, s), 1 + phase, 0.6 if phase else 0.75, after + [("clear_padding",)], over_pair(kind, s))
+        for q in range(len(lasts)):
+            tag = [("s", phase, q, i) for i in range(5)]
+            act(("sum_start", phase, q), -4, 0.02, [("project", phase, lasts[q])], (), [("m", 4 * chunk, tag[0])])
+            sends = [("x0", chunk / 2, tag[1]), ("x1", chunk / 2, tag[2])]
+            act(("sum_chip", phase, q), -5, 0.16, [("sum_start", phase, q)], tag[:1], sends)
+            sends = [("x0", chunk, tag[3]), ("x1", chunk, tag[4])]
+            act(("sum_on", phase, q), -6, 0.06, [("sum_chip", phase, q)], tag[1:3], sends)
+            after = [("sum_on", phase, q)]
+            if phase:
+                act(("updated", q), -1, 0.2, after, tag[3:])
+            else:
+                sends = gather(1 + q, chunk, ("after_first", q), -8)
+                act(("after_first", q), -7, 0.14, after, tag[3:], sends)
+    for s in range(1, half + 1):
+        after = [("gather_mate", 1 + min(q for q, last in enumerate(lasts) if s <= last)), ("z_event", 2, 0, s), ("z_event", 2, 1, s)]
+        after.append(("qkv_compute", s - 1) if s > 1 else ("hidden",))
+        act(("qkv_compute", s), 1.5, 0.92, after, over_pair(2, s))
+    act(("qkv_end",), 0, 0.67, [("qkv_compute", half)])
+    act(("retention",), 0, 3.1, [("qkv_end",)] + decays)
+    return acts
+
+
+def in_order(acts, trace=None):
+    arrival, free, done, left, now = {}, {}, set(), dict(acts), 0.0
+    while left:
+        ready = []
+        for place, (name, (rank, _, after, need, _)) in enumerate(left.items()):
+            if all(v in done for v in after) and all(v in arrival for v in need):
+                ready.append((max([now] + [arrival[v] for v in need]), rank, place, name))
+        begin, _, _, name = min(ready)
+        _, time, _, _, sends = left.pop(name)
+        if trace is not None:
+            trace.append((name, now, begin))
+        now = begin + time
+        done.add(name)
+        for link, nbytes, tag in sends:
+            free[link] = max(free.get(link, 0.0), now) + nbytes / (MATE if link == "m" else LINK)
+            arrival[tag] = free[link] + LATENCY[link]
+        yield name
 
 
 def half_mask(tile):
@@ -90,10 +199,10 @@
     odd = lax.rem(g, 2)
     g_mate = g + 1 - 2 * odd
     rows = x1.shape[1]
-    ff = gate_in.shape[1]
+    ff = gate_in.shape[0]
     main = ff // LANES * LANES
-    tail = ff - main
     started = []
+    per = STEP_TILE // LANES // 2
 
     def remote(src, dst, ss_, rs_, **to):
         return pltpu.make_async_remote_copy(
@@ -115,6 +224,9 @@
         copy.start()
         local.append(copy)
 
+    for i, weight in enumerate((gate_in, up_in)):
+        fetch(weight.at[pl.ds(0, main)], gu.at[me, pl.ds(i * main, main)])
+        fetch(weight.at[pl.ds(main, ff - main)], gu.at[me, pl.ds(2 * main + i * (ff - main), ff - main)])
     fetch(tok_in, x1.at[r])
     fetch(down_in, dn.at[me, pl.ds(0, ff)])
     dk, dv = q_in.shape[1], v_in.shape[1]
@@ -122,10 +234,6 @@
     fetch(k_in, qkv.at[me, :, pl.ds(dk, dk)])
     fetch(v_in, qkv.at[me, :, pl.ds(2 * dk, dv)])
     fetch(out_in, wo.at[me])
-
-    gu[me, :, :main] = gate_in[:, :main]
-    gu[me, :, main : 2 * main] = up_in[:, :main]
-    gu[me, :, 2 * main :] = jnp.concatenate([gate_in[:, main:], up_in[:, main:]], axis=1)
 
     barrier = pltpu.get_barrier_semaphore()
     neighbours = [
@@ -138,9 +246,11 @@
     ]
     for to in neighbours:
         pl.semaphore_signal(barrier, inc=1, device_id=to, device_id_type=MESH)
-    pl.semaphore_wait(barrier, len(neighbours))
-    for copy in local:
-        copy.wait()
+    with jax.named_scope("entry"):
+        pl.semaphore_wait(barrier, len(neighbours))
+    with jax.named_scope("fetched"):
+        for copy in local:
+            copy.wait()
 
     kinds = (gu, dn, qkv, wo)
     lengths = (gu.shape[1], ff, qkv.shape[1], wo.shape[1])
@@ -163,8 +273,8 @@
     def after(s):
         return lax.rem(me + s, n)
 
-    def hops(sub, way):
-        return half if sub == way else half - 1
+    def hops(kind, way):
+        return half - SHORTER[kind][way]
 
     def z_start(kind, sub, way, s):
         block = before(s) if way == 0 else after(s)
@@ -174,22 +284,30 @@
 
     def z_event(kind, sub, s):
         for way in range(2):
-            if s > hops(sub, way):
+            if s > hops(kind, way):
                 continue
             block = before(s) if way == 0 else after(s)
             ref = kinds[kind].at[block, z_rows(kind, sub)]
             slot = (2 * kind + sub, way, s - 1)
             arrived(ref, z_send.at[slot], z_recv.at[slot], fs=down_z if way == 0 else up_z)
-            if s < hops(sub, way):
+            if s < hops(kind, way):
                 z_start(kind, sub, way, s)
-            if sub == 0:
-                ref = kinds[kind].at[block, y_rows(kind, True)]
-                slot = (kind, way, s - 1)
-                send(ref, ref, y_send.at[slot], y_recv.at[slot], grp=g_mate)
+    def y_start(kind, s):
+        for way in range(2):
+            if s > hops(kind, way):
+                continue
+            block = before(s) if way == 0 else after(s)
+            ref = kinds[kind].at[block, y_rows(kind, True)]
+            slot = (kind, way, s - 1)
+            send(ref, ref, y_send.at[slot], y_recv.at[slot], grp=g_mate)
+
+    def z_own(kind, sub):
+        for way in range(2):
+            z_start(kind, sub, way, 0)
 
     def y_wait(kind, s):
         for way in range(2):
-            if s > hops(0, way):
+            if s > hops(kind, way):
                 continue
             block = before(s) if way == 0 else after(s)
             ref = kinds[kind].at[block, y_rows(kind, False)]
@@ -270,7 +388,6 @@
         return pl.ds(pl.multiple_of(block * LANES, LANES), LANES)
 
     def blocks_of(q):
-        per = STEP_TILE // LANES // 2
         return [b for s in range(q * per + 1, (q + 1) * per + 1) for b in pair_of(s)]
 
     def after_first(q):
@@ -315,8 +432,8 @@
         def step(m):
             part = pl.ds(pl.multiple_of(m * tile, tile), tile)
             left = jnp.concatenate([x1n[a, part], x1n[b, part]], axis=1)
-            right = jnp.concatenate([gu[a], gu[b]], axis=0)
-            product = jnp.dot(left, right, preferred_element_type=F32)
+            right = jnp.concatenate([gu[a], gu[b]], axis=1)
+            product = lax.dot_general(left, right, (((1,), (1,)), ((), ())), preferred_element_type=F32)
             acc[part] = product if s == 1 else acc[part] + product
 
         tiles(step)
@@ -340,7 +457,7 @@
         y_wait(kind, s)
         a, b = pair_of(s)
         w = kinds[kind]
-        q, at = (s - 1) // 2, (s - 1) % 2 * 2 * LANES
+        q, at = (s - 1) // per, (s - 1) % per * 2 * LANES
 
         def step(m):
             part = pl.ds(pl.multiple_of(m * tile, tile), tile)
@@ -355,14 +472,14 @@
     def qkv_compute(s):
         y_wait(2, s)
         a, b = pair_of(s)
-        q, at = (s - 1) // 2, (s - 1) % 2 * 2 * LANES
+        q, at = (s - 1) // per, (s - 1) % per * 2 * LANES
         gain = jnp.concatenate([gain2[:, block_lanes(a)], gain2[:, block_lanes(b)]], axis=1)
-        per = tile // rows
+        count = tile // rows
         width = qkv.shape[2]
 
         def step(m):
             part = pl.ds(pl.multiple_of(m * tile, tile), tile)
-            value = x2[q, pl.ds(m * per, per), :, at : at + 2 * LANES].reshape(tile, 2 * LANES).astype(F32)
+            value = x2[q, pl.ds(m * count, count), :, at : at + 2 * LANES].reshape(tile, 2 * LANES).astype(F32)
             square = value * value
             square = square[:, :LANES] + square[:, LANES:]
             right = jnp.concatenate([qkv[a], qkv[b]], axis=0)
@@ -387,7 +504,7 @@
 
     def make_decay(first, last):
         size = seq // 8
-        forward, backward = rates[0, 0], rates[1, 0]
+        forward, backward = rates[0, 0], rates[0, 1]
 
         def body(m, carry):
             at = lax.broadcasted_iota(jnp.int32, (size, seq), 0) + m * size
@@ -422,80 +539,46 @@
         if pad:
             lax.fori_loop(0, n, body, 0)
 
-    plan = []
-
-    def at(place, what, *args):
-        plan.append((place, len(plan), functools.partial(what, *args)))
-
-    def ring_starts(place, kind, sub):
-        for way in range(2):
-            at(place, z_start, kind, sub, way, 0)
-
-    place = {}
-    order = [(0, sub, s) for s in range(1, half + 1) for sub in range(2)]
-    for s in range(1, half + 1):
-        order += [(1, 0, s), (2, 0, s), (1, 1, s)]
-    lag = 3
-    for slot in range(1, half + 1 + lag):
-        if slot <= half:
-            order.append((2, 1, slot))
-        if slot > lag:
-            order += [(3, 0, slot - lag), (3, 1, slot - lag)]
-    for i, event in enumerate(order):
-        place[event] = i
-        at(i, z_event, *event)
-    for kind in range(4):
-        for sub in range(2):
-            ring_starts(-1 if kind == 0 else place[kind, sub, 1] - 2.5, kind, sub)
-
-    at(-0.9, gather_start, x1_buf, 0)
-    at(-0.5, clear_padding)
-    for i in range(4):
-        at(0.5 + i, make_decay, 2 * i, 2 * i + 2)
-    at(4.5, gather_on, x1_buf, 0, rows)
-    at(6.5, gather_far, x1_buf, 0, rows)
-    at(7.5, gather_mate, x1_buf, 0)
-    at(7.6, norm_tokens, 0, 4)
-    at(8.6, norm_tokens, 4, 8)
-    when = 9.5
-    for s in range(1, half + 1):
-        when = max(when + 0.5, place[0, 1, s] + 1.5)
-        at(when, gu_compute, s)
-    at(when + 0.1, hidden)
-    when += 0.2
-    chunks = d // STEP_TILE
-    per = half // chunks
-    gathered = []
-    for q in range(chunks):
-        for s in range(q * per + 1, (q + 1) * per + 1):
-            when = max(when + 0.5, place[1, 1, s] + 1.5)
-            at(when, project, 1, s, hid, p1)
-        at(when + 0.1, sum_start, 0, q)
-        at(when + 2.2, sum_chip, 0, q)
-        at(when + 5.2, sum_on, 0, q)
-        at(when + 8.2, after_first, q)
-        at(when + 11.2, gather_on, x2_buf(q), 1 + q, rows)
-        at(when + 13.2, gather_far, x2_buf(q), 1 + q, rows)
-        at(when + 14.2, gather_mate, x2_buf(q), 1 + q)
-        gathered.append(when + 14.2)
-    when = 0
-    for s in range(1, half + 1):
-        when = max(when + 0.5, place[2, 1, s] + 1.5, gathered[(s - 1) // per] + 0.1)
-        at(when, qkv_compute, s)
-    at(when + 0.1, qkv_end)
-    at(when + 0.2, retention)
-    when += 0.3
-    for q in range(chunks):
-        for s in range(q * per + 1, (q + 1) * per + 1):
-            when = max(when + 0.5, place[3, 1, s] + 1.5)
-            at(when, project, 3, s, hn, p2)
-        at(when + 0.1, sum_start, 1, q)
-        at(when + 1.2, sum_chip, 1, q)
-        at(when + 2.2, sum_on, 1, q)
-        at(when + 3.2, updated, q)
-
-    for _, _, what in sorted(plan, key=lambda entry: entry[:2]):
-        what()
+    sizes = {
+        "half": half,
+        "parts": parts,
+        "row_bytes": [k.shape[2] * 2 for k in kinds],
+        "hops": [[hops(kind, way) for way in range(2)] for kind in range(4)],
+        "tok_bytes": rows * d * 2,
+        "per": per,
+        "chunk_bytes": rows * STEP_TILE * 2,
+    }
+    steps = {
+        "z_own": z_own,
+        "z_event": z_event,
+        "y_start": y_start,
+        "gather_start": lambda k: gather_start(x1_buf, k),
+        "gather_on": lambda k: gather_on(x2_buf(k - 1) if k else x1_buf, k, rows),
+        "gather_far": lambda k: gather_far(x2_buf(k - 1) if k else x1_buf, k, rows),
+        "gather_mate": lambda k: gather_mate(x2_buf(k - 1) if k else x1_buf, k),
+        "clear_padding": clear_padding,
+        "make_decay": make_decay,
+        "norm_tokens": norm_tokens,
+        "gu_compute": gu_compute,
+        "hidden": hidden,
+        "project": lambda phase, s: project(3, s, hn, p2) if phase else project(1, s, hid, p1),
+        "sum_start": sum_start,
+        "sum_chip": sum_chip,
+        "sum_on": sum_on,
+        "after_first": after_first,
+        "updated": updated,
+        "qkv_compute": qkv_compute,
+        "qkv_end": qkv_end,
+        "retention": retention,
+    }
+    order = list(in_order(actions(sizes)))
+    for i, (name, *args) in enumerate(order):
+        if i == len(order) - 1:
+            early, started[:] = started[:-8], started[-8:]
+            for copy in early:
+                copy.wait_send()
+        with jax.named_scope(name):
+            steps[name](*args)
     for copy in started:
         copy.wait_send()
 
@@ -505,7 +588,8 @@
 
     def shards(tokens, g1, g2, gate, up, down, query, key, value, head_gain, out, log_decay):
         rows, d = tokens.shape
-        ff = gate.shape[1]
+        gate, up, log_decay = gate.T, up.T, log_decay.T
+        ff = gate.shape[0]
         dk, dv = query.shape[1], value.shape[1]
         seq = rows * n_tp
         chunks = d // STEP_TILE
@@ -523,10 +607,10 @@
         return pl.pallas_call(
             functools.partial(kernel, (n, groups)),
             out_shape=jax.ShapeDtypeStruct((rows, d), BF16),
-            in_specs=[hbm, vmem, vmem, vmem, vmem, hbm, hbm, hbm, hbm, vmem, hbm, pl.BlockSpec(memory_space=pltpu.SMEM)],
+            in_specs=[hbm, vmem, vmem, hbm, hbm, hbm, hbm, hbm, hbm, vmem, hbm, pl.BlockSpec(memory_space=pltpu.SMEM)],
             out_specs=vmem,
             scratch_shapes=[
-                pltpu.VMEM((n, LANES, 2 * ff), BF16),
+                pltpu.VMEM((n, 2 * ff, LANES), BF16),
                 pltpu.VMEM((n, ff_pad, LANES), BF16),
                 pltpu.VMEM((n, LANES, 2 * dk + dv), BF16),
                 pltpu.VMEM((n, dv, LANES), BF16),
@@ -551,7 +635,7 @@
                 dma((2, chunks, 5)),
                 dma((1 + chunks, 8)),
                 dma((1 + chunks, 8)),
-                dma((6,)),
+                dma((10,)),
             ],
             compiler_params=pltpu.CompilerParams(
                 collective_id=0, has_side_effects=True, vmem_limit_bytes=67_000_000

time: 195 us -> 156 us (0.80)
  Pallas kernels: 189 us -> 154 us
  local copies, waits for them, and re-layouts: 5.72 us -> 1.88 us
    pallas_call x1, Pallas kernels: 189 us -> 154 us  [shards(): pl.pallas_call(functools.partial(kernel, (n, groups)), out_shape=jax.Shap...]
    unnamed x8 -> x1, local copies, waits for them, and re-layouts: 5.72 us -> 1.88 us
where the time goes in v2:
time: 156 us
  Pallas kernels  154 us (99%)
  local copies, waits for them, and re-layouts  1.88 us (1%)
    pallas_call x1, Pallas kernels, shards(): pl.pallas_call(functools.partial(kernel, (n, groups)), out_shape=jax.Shap...  154 us

profile of v2, /device:TPU:33, one launch (start us, length us, event | category | flops | bytes accessed | tf_op | source)
XLA Modules:
  0.0 156.2 jit_solution(5723174118858611749)
XLA Ops:
  0.0 154.3 %shard_map.118 = bf16[128,2048]{1,0:T(8,128)(2,1)} custom-call(bf16[128,2048]{1,0:T(8,128)(2,1)} %tok_in.1, f32[1,2048]{1,0:T(1,128)} %bitcast.8, f32[1,2048]{1,0:T(1,128)} %bitcast.9, bf16[576,128]{1,0:T(8,128)(2,1)} %bitcast.6, bf16[576,128]{1,0:T(8,128)(2,1)} %bitcast.7, bf16[576,128]{1,0:T(8,128)(2,1)} %down_in.1, bf16[128,256]{1,0:T(8,128)(2,1)} %q_in.1, ...), custom_call_target="tpu_custom_call" | custom-call | tf_op jit(solution)/shard_map/pallas_call | solution.py:607
  154.3 1.9 %copy.14 = bf16[128,2048]{1,0:T(8,128)(2,1)} copy(bf16[128,2048]{1,0:T(8,128)(2,1)} %shard_map.118) | data formatting | bytes 1048576

commit v3 on v2

--- a/solution.py
+++ b/solution.py
@@ -14,18 +14,20 @@
 ROW_TILE = 16
 STEP_TILE = 256
 SHORTER = ((0, 1), (1, 0), (0, 1), (0, 1))
-PAIR_SHARE = (0.36, 0.43, 0.36, 0.36)
-RING_STARTS = ((((0, 0, 4),), ((0, 0, 6),)), (((1, 1, 2),), ((1, 1, 3),)), (((2, 0, 5),), ((1, 1, 8),)))
-RANKS = {}
-GU_TIME = 1.07
+PAIR_SHARE = (0.376, 0.334, 0.25, 0.4)
+PIECES = (3, 2, 3, 2)
+RING_STARTS = ((((0, 1, 4),), ((0, 1, 5),)), (((1, 0, 3),), ((1, 0, 4),), ((1, 1, 4),)), (((2, 2, 4),), ((2, 0, 4),)))
+RANKS = {'project': -3, 'qkv_compute': 2, 'gather_on': -1, 'gather_far': -12, 'gather_mate': -3, 'sum_start': -8, 'sum_chip': -1, 'sum_on': -4, 'after_first': 0, 'updated': -12, 'gu_compute': -2, 'out_start': -25, 'out_chip': -5, 'out_on': -1}
+GU_TIME, KEEP_TIME, OUT_TIMES = 1.07, 0.8, (0.28, 0.47)
 LINK, MATE = 46650.0, 600000.0
-LATENCY = {"z0": 2.0, "z1": 2.0, "x0": 2.0, "x1": 2.0, "m": 1.1, "y": 2.0}
-
-
-def split_rows(rows, share):
-    pair = int(rows * share) // ROW_TILE * ROW_TILE
-    first = max(-(-(rows - pair) // (2 * ROW_TILE)) * ROW_TILE, pair)
-    return first, rows - pair - first, pair
+LATENCY = {"z0": 2.6, "z1": 2.6, "x0": 2.8, "x1": 2.8, "m": 1.0, "y": 3.0}
+
+
+def split_rows(rows, share, pieces):
+    pair = int(rows * share) // ROW_TILE
+    units = rows // ROW_TILE - pair
+    cuts = [-(-units * i // pieces) * ROW_TILE for i in range(pieces + 1)]
+    return tuple(b - a for a, b in zip(cuts, cuts[1:])) + (pair * ROW_TILE,)
 
 
 def actions(sizes):
@@ -43,9 +45,14 @@
     def over_pair(kind, s):
         return [("y", kind, w, s) for w in ways(kind, s)]
 
+    def landed(kind, s):
+        return [("z_event", kind, sub, s) for sub in range(len(parts[kind]) - 1)]
+
     for kind in range(4):
         nbytes = [rows * row_bytes[kind] for rows in parts[kind]]
-        for sub in range(2):
+        subs = len(nbytes) - 1
+        covered = min(sub for sub in range(subs) if sum(parts[kind][: sub + 1]) >= parts[kind][-1])
+        for sub in range(subs):
             after = [("z_event", *v) for v in RING_STARTS[kind - 1][sub]] if kind else []
             own = [(f"z{w}", nbytes[sub], ("z", kind, sub, w, 1)) for w in range(2)]
             act(("z_own", kind, sub), -10 + 0.1 * kind, 0.03, after, (), own)
@@ -55,10 +62,10 @@
                 after = [("z_event", kind, sub, s - 1) if s > 1 else ("z_own", kind, sub)]
                 act(("z_event", kind, sub, s), -20 + kind, 0.05, after, need, onward)
         for s in range(1, half + 1):
-            after = [("z_event", kind, 0, s)]
+            after = [("z_event", kind, sub, s) for sub in range(covered + 1)]
             if s > 1 or kind:
                 after.append(("y_start", kind, s - 1) if s > 1 else ("y_start", kind - 1, half))
-            act(("y_start", kind, s), -15 + kind, 0.02, after, (), [("y", nbytes[2], v) for v in over_pair(kind, s)])
+            act(("y_start", kind, s), -15 + kind, 0.02, after, (), [("y", nbytes[-1], v) for v in over_pair(kind, s)])
 
     def gather(k, nbytes, first, rank):
         on = [("x0", nbytes / 2, 3), ("m", nbytes, 5), ("x1", nbytes / 2, 4), ("m", nbytes, 6)]
@@ -81,34 +88,42 @@
     for name in norms:
         act(name, -3, 0.92, [("gather_mate", 0)])
     for s in range(1, half + 1):
-        after = [("z_event", 0, sub, s) for sub in range(2)] + (norms if s == 1 else [("gu_compute", s - 1)])
+        after = landed(0, s) + (norms if s == 1 else [("gu_compute", s - 1)])
         act(("gu_compute", s), 0, GU_TIME, after, over_pair(0, s))
     act(("hidden",), 0, 0.85, [("gu_compute", half)])
-    for phase in range(2):
-        kind = 3 if phase else 1
-        first = ("retention",) if phase else ("hidden",)
-        for s in range(1, half + 1):
-            after = [("z_event", kind, sub, s) for sub in range(2)] + [("project", phase, s - 1) if s > 1 else first]
-            act(("project", phase, s), 1 + phase, 0.6 if phase else 0.75, after + [("clear_padding",)], over_pair(kind, s))
+    for q in range(len(lasts)):
+        tag = [("s", 0, q, i) for i in range(5)]
+        for s in range(lasts[q] - per + 1, lasts[q] + 1):
+            after = landed(1, s) + [("project", s - 1) if s > 1 else ("hidden",), ("clear_padding",)]
+            act(("project", s), 1, 0.75, after, over_pair(1, s))
+        act(("sum_start", q), -4, 0.02, [("project", lasts[q])], (), [("m", 4 * chunk, tag[0])])
+        sends = [("x0", chunk / 2, tag[1]), ("x1", chunk / 2, tag[2])]
+        act(("sum_chip", q), -5, 0.16, [("sum_start", q)], tag[:1], sends)
+        sends = [("x0", chunk, tag[3]), ("x1", chunk, tag[4])]
+        act(("sum_on", q), -6, 0.06, [("sum_chip", q)], tag[1:3], sends)
+        sends = gather(1 + q, chunk, ("after_first", q), -8)
+        act(("after_first", q), -7, 0.14, [("sum_on", q)], tag[3:], sends)
+    for m in range(4):
+        act(("keep", m), 0 if m == 0 else 3, KEEP_TIME, [("keep", m - 1) if m else ("qkv_end",)] + decays)
+    for m, time in enumerate(OUT_TIMES):
         for q in range(len(lasts)):
-            tag = [("s", phase, q, i) for i in range(5)]
-            act(("sum_start", phase, q), -4, 0.02, [("project", phase, lasts[q])], (), [("m", 4 * chunk, tag[0])])
-            sends = [("x0", chunk / 2, tag[1]), ("x1", chunk / 2, tag[2])]
-            act(("sum_chip", phase, q), -5, 0.16, [("sum_start", phase, q)], tag[:1], sends)
-            sends = [("x0", chunk, tag[3]), ("x1", chunk, tag[4])]
-            act(("sum_on", phase, q), -6, 0.06, [("sum_chip", phase, q)], tag[1:3], sends)
-            after = [("sum_on", phase, q)]
-            if phase:
-                act(("updated", q), -1, 0.2, after, tag[3:])
-            else:
-                sends = gather(1 + q, chunk, ("after_first", q), -8)
-                act(("after_first", q), -7, 0.14, after, tag[3:], sends)
+            tags = [("s", 1, q, 5 + i) for i in ((1, 2, 3) if m else (0,))]
+            for s in range(lasts[q] - per + 1, lasts[q] + 1):
+                after = landed(3, s) + [("out", s - 1, m) if s > 1 else ("keep", 3 * m)] + [("out", s, 0)] * m
+                act(("out", s, m), 2 + 2 * m, time, after, over_pair(3, s))
+            act(("out_start", q, m), -4, 0.03, [("out", lasts[q], m)], (), [("m", chunk, tag) for tag in tags])
+            sends = [] if m else [("x0", chunk / 2, ("s", 1, q, 1)), ("x1", chunk / 2, ("s", 1, q, 2))]
+            act(("out_chip", q, m), -5, 0.05, [("out_start", q, m)], tags, sends)
+    for q in range(len(lasts)):
+        tag = [("s", 1, q, i) for i in range(5)]
+        sends = [("x0", chunk, tag[3]), ("x1", chunk, tag[4])]
+        act(("out_on", q), -6, 0.06, [("out_chip", q, 0), ("out_chip", q, 1)], tag[1:3], sends)
+        act(("updated", q), -1, 0.2, [("out_on", min(q + 4, len(lasts) - 1))], tag[3:])
     for s in range(1, half + 1):
-        after = [("gather_mate", 1 + min(q for q, last in enumerate(lasts) if s <= last)), ("z_event", 2, 0, s), ("z_event", 2, 1, s)]
+        after = [("gather_mate", 1 + min(q for q, last in enumerate(lasts) if s <= last))] + landed(2, s)
         after.append(("qkv_compute", s - 1) if s > 1 else ("hidden",))
         act(("qkv_compute", s), 1.5, 0.92, after, over_pair(2, s))
     act(("qkv_end",), 0, 0.67, [("qkv_compute", half)])
-    act(("retention",), 0, 3.1, [("qkv_end",)] + decays)
     return acts
 
 
@@ -254,16 +269,15 @@
 
     kinds = (gu, dn, qkv, wo)
     lengths = (gu.shape[1], ff, qkv.shape[1], wo.shape[1])
-    parts = [split_rows(length, share) for length, share in zip(lengths, PAIR_SHARE)]
+    parts = [split_rows(*v) for v in zip(lengths, PAIR_SHARE, PIECES)]
 
     def z_rows(kind, sub):
-        first, second, pair = parts[kind]
-        if sub == 0:
-            return pl.ds(pl.multiple_of(odd * (lengths[kind] - first), ROW_TILE), first)
-        return pl.ds(pl.multiple_of(first + odd * (pair - first), ROW_TILE), second)
+        size, start = parts[kind][sub], sum(parts[kind][:sub])
+        mirrored = lengths[kind] - start - size
+        return pl.ds(pl.multiple_of(start + odd * (mirrored - start), ROW_TILE), size)
 
     def y_rows(kind, sent):
-        pair = parts[kind][2]
+        pair = parts[kind][-1]
         at = odd if sent else 1 - odd
         return pl.ds(pl.multiple_of(at * (lengths[kind] - pair), ROW_TILE), pair)
 
@@ -279,7 +293,7 @@
     def z_start(kind, sub, way, s):
         block = before(s) if way == 0 else after(s)
         ref = kinds[kind].at[block, z_rows(kind, sub)]
-        slot = (2 * kind + sub, way, s)
+        slot = (sum(PIECES[:kind]) + sub, way, s)
         send(ref, ref, z_send.at[slot], z_recv.at[slot], fs=up_z if way == 0 else down_z)
 
     def z_event(kind, sub, s):
@@ -288,7 +302,7 @@
                 continue
             block = before(s) if way == 0 else after(s)
             ref = kinds[kind].at[block, z_rows(kind, sub)]
-            slot = (2 * kind + sub, way, s - 1)
+            slot = (sum(PIECES[:kind]) + sub, way, s - 1)
             arrived(ref, z_send.at[slot], z_recv.at[slot], fs=down_z if way == 0 else up_z)
             if s < hops(kind, way):
                 z_start(kind, sub, way, s)
@@ -351,28 +365,50 @@
 
         return buf
 
-    def sum_start(phase, q):
+    sides = ((r_left, r_right, xr), (r_right, r_left, xl))
+
+    def on_mate(phase, q, i, to):
         p_, r_ = (p1, r1) if phase == 0 else (p2, r2)
-        send(p_.at[q, 1 - c], r_.at[q], x_send.at[phase, q, 0], x_recv.at[phase, q, 0], tp=r_mate)
-
-    def sum_chip(phase, q):
-        p_, r_, s_, h_ = (p1, r1, s1, h1) if phase == 0 else (p2, r2, s2, h2)
-        arrived(r_.at[q], x_send.at[phase, q, 0], x_recv.at[phase, q, 0], tp=r_mate)
-
-        def add(to):
-            s_[q, to] = (p_[q, c, to].astype(F32) + r_[q, to].astype(F32)).astype(BF16)
-
-        add(xo)
+        return p_.at[q, 1 - c, to], r_.at[q, to], x_send.at[phase, q, i], x_recv.at[phase, q, i]
+
+    def add_mate(phase, q, to):
+        p_, r_, s_ = (p1, r1, s1) if phase == 0 else (p2, r2, s2)
+        s_[q, to] = (p_[q, c, to].astype(F32) + r_[q, to].astype(F32)).astype(BF16)
+
+    def send_halves(phase, q):
+        s_, h_ = (s1, h1) if phase == 0 else (s2, h2)
         for i, to in enumerate((r_right, r_left)):
             part = pl.ds(i * (rows // 2), rows // 2)
             send(s_.at[q, xo, part], h_.at[q, i], x_send.at[phase, q, 1 + i], x_recv.at[phase, q, 1 + i], tp=to)
-        add(xr)
-        add(xl)
-        add(x)
+
+    def sum_start(q):
+        send(p1.at[q, 1 - c], r1.at[q], x_send.at[0, q, 0], x_recv.at[0, q, 0], tp=r_mate)
+
+    def sum_chip(q):
+        arrived(r1.at[q], x_send.at[0, q, 0], x_recv.at[0, q, 0], tp=r_mate)
+        add_mate(0, q, xo)
+        send_halves(0, q)
+        for to in (xr, xl, x):
+            add_mate(0, q, to)
+
+    chips = (xo, xr, xl, x)
+
+    def out_start(q, m):
+        for i in (1, 2, 3) if m else (0,):
+            src, dst, *sems = on_mate(1, q, 5 + i, chips[i])
+            send(src, dst, *sems, tp=r_mate)
+
+    def out_chip(q, m):
+        for i in (1, 2, 3) if m else (0,):
+            _, dst, *sems = on_mate(1, q, 5 + i, chips[i])
+            arrived(dst, *sems, tp=r_mate)
+            add_mate(1, q, chips[i])
+        if m == 0:
+            send_halves(1, q)
 
     def sum_on(phase, q):
         s_, h_, f_ = (s1, h1, f1) if phase == 0 else (s2, h2, f2)
-        for i, (src, to, x_to) in enumerate(((r_left, r_right, xr), (r_right, r_left, xl))):
+        for i, (src, to, x_to) in enumerate(sides):
             arrived(h_.at[q, i], x_send.at[phase, q, 1 + i], x_recv.at[phase, q, 1 + i], tp=src)
             part = pl.ds(i * (rows // 2), rows // 2)
             s_[q, x_to, part] = (s_[q, x_to, part].astype(F32) + h_[q, i].astype(F32)).astype(BF16)
@@ -453,21 +489,32 @@
 
         tiles(step, 8)
 
-    def project(kind, s, left, p_):
-        y_wait(kind, s)
+    def project(s):
+        y_wait(1, s)
         a, b = pair_of(s)
-        w = kinds[kind]
         q, at = (s - 1) // per, (s - 1) % per * 2 * LANES
 
         def step(m):
             part = pl.ds(pl.multiple_of(m * tile, tile), tile)
-            right = jnp.concatenate([w[a], w[b]], axis=1)
-            product = jnp.dot(left[part], right, preferred_element_type=F32).astype(BF16)
+            right = jnp.concatenate([dn[a], dn[b]], axis=1)
+            product = jnp.dot(hid[part], right, preferred_element_type=F32).astype(BF16)
             for i in range(tile // rows):
                 to = m * (tile // rows // 2) + i // 2
-                p_[q, i % 2, to, :, at : at + 2 * LANES] = product[i * rows : (i + 1) * rows]
+                p1[q, i % 2, to, :, at : at + 2 * LANES] = product[i * rows : (i + 1) * rows]
 
         tiles(step)
+
+    def out(s, m):
+        if m == 0:
+            y_wait(3, s)
+        a, b = pair_of(s)
+        q, at = (s - 1) // per, (s - 1) % per * 2 * LANES
+        first, last = (1, 4) if m else (0, 1)
+        left = hn[first * 2 * rows : last * 2 * rows]
+        right = jnp.concatenate([wo[a], wo[b]], axis=1)
+        product = jnp.dot(left, right, preferred_element_type=F32).astype(BF16)
+        for i in range(2 * (last - first)):
+            p2[q, i % 2, chips[first + i // 2], :, at : at + 2 * LANES] = product[i * rows : (i + 1) * rows]
 
     def qkv_compute(s):
         y_wait(2, s)
@@ -516,18 +563,13 @@
 
         lax.fori_loop(first, last, body, 0)
 
-    def retention():
-        size = seq // 4
-
-        def step(m):
-            part = pl.ds(pl.multiple_of(m * size, size), size)
-            score = lax.dot_general(qs[part], ks[...], (((1,), (1,)), ((), ())), preferred_element_type=F32)
-            kept = jnp.dot((score * decay[part]).astype(BF16), vs[...], preferred_element_type=F32)
-            kept = kept - jnp.mean(kept, axis=1, keepdims=True)
-            variance = jnp.mean(kept * kept, axis=1, keepdims=True)
-            hn[part] = (kept * lax.rsqrt(variance + EPS) * hgain[...]).astype(BF16)
-
-        tiles(step, 4)
+    def keep(m):
+        part = pl.ds(pl.multiple_of(chips[m] * 2 * rows, 2 * rows), 2 * rows)
+        score = lax.dot_general(qs[part], ks[...], (((1,), (1,)), ((), ())), preferred_element_type=F32)
+        kept = jnp.dot((score * decay[part]).astype(BF16), vs[...], preferred_element_type=F32)
+        kept = kept - jnp.mean(kept, axis=1, keepdims=True)
+        variance = jnp.mean(kept * kept, axis=1, keepdims=True)
+        hn[m * 2 * rows : (m + 1) * 2 * rows] = (kept * lax.rsqrt(variance + EPS) * hgain[...]).astype(BF16)
 
     def clear_padding():
         pad = dn.shape[1] - ff
@@ -561,15 +603,19 @@
         "norm_tokens": norm_tokens,
         "gu_compute": gu_compute,
         "hidden": hidden,
-        "project": lambda phase, s: project(3, s, hn, p2) if phase else project(1, s, hid, p1),
+        "project": project,
         "sum_start": sum_start,
         "sum_chip": sum_chip,
-        "sum_on": sum_on,
+        "sum_on": lambda q: sum_on(0, q),
+        "keep": keep,
+        "out": out,
+        "out_start": out_start,
+        "out_chip": out_chip,
+        "out_on": lambda q: sum_on(1, q),
         "after_first": after_first,
         "updated": updated,
         "qkv_compute": qkv_compute,
         "qkv_end": qkv_end,
-        "retention": retention,
     }
     order = list(in_order(actions(sizes)))
     for i, (name, *args) in enumerate(order):
@@ -627,12 +673,12 @@
                 pltpu.VMEM((seq, seq), F32),
                 pltpu.VMEM((seq, dv), BF16),
                 pltpu.VMEM((seq, LANES), F32),
-                dma((8, 2, n // 2)),
-                dma((8, 2, n // 2)),
+                dma((sum(PIECES), 2, n // 2)),
+                dma((sum(PIECES), 2, n // 2)),
                 dma((4, 2, n // 2)),
                 dma((4, 2, n // 2)),
-                dma((2, chunks, 5)),
-                dma((2, chunks, 5)),
+                dma((2, chunks, 9)),
+                dma((2, chunks, 9)),
                 dma((1 + chunks, 8)),
                 dma((1 + chunks, 8)),
                 dma((10,)),

time: 156 us -> 155 us (level)
  Pallas kernels: 154 us -> 152 us
    pallas_call x1, Pallas kernels: 154 us -> 152 us  [shards(): pl.pallas_call(functools.partial(kernel, (n, groups)), out_shape=jax.Shap...]
where the time goes in v3:
time: 155 us; the launch traced here: 154 us
  Pallas kernels  152 us (98%)
  local copies, waits for them, and re-layouts  1.88 us (1%)
    pallas_call x1, Pallas kernels, shards(): pl.pallas_call(functools.partial(kernel, (n, groups)), out_shape=jax.Shap...  152 us

profile of v3, /device:TPU:33, one launch (start us, length us, event | category | flops | bytes accessed | tf_op | source)
XLA Modules:
  0.0 154.3 jit_solution(14557804760708808012)
XLA Ops:
  0.0 152.4 %shard_map.118 = bf16[128,2048]{1,0:T(8,128)(2,1)} custom-call(bf16[128,2048]{1,0:T(8,128)(2,1)} %tok_in.1, f32[1,2048]{1,0:T(1,128)} %bitcast.8, f32[1,2048]{1,0:T(1,128)} %bitcast.9, bf16[576,128]{1,0:T(8,128)(2,1)} %bitcast.6, bf16[576,128]{1,0:T(8,128)(2,1)} %bitcast.7, bf16[576,128]{1,0:T(8,128)(2,1)} %down_in.1, bf16[128,256]{1,0:T(8,128)(2,1)} %q_in.1, ...), custom_call_target="tpu_custom_call" | custom-call | tf_op jit(solution)/shard_map/pallas_call | solution.py:653
  152.5 1.9 %copy.14 = bf16[128,2048]{1,0:T(8,128)(2,1)} copy(bf16[128,2048]{1,0:T(8,128)(2,1)} %shard_map.118) | data formatting | bytes 1048576
